TPU v7x, 32 devices: a whole 2x2x4 slice. The times are simulated.
32 devices in a mesh: grp: 2 (over x), kv: 4 (over z), tp: 4 (over y, core).
Axes of the slice: x: 2, y: 2, z: 4, core: 2. Of those that a mesh axis runs over, the one named last changes fastest.
Arguments:
- x_rows: bfloat16 [256, 4096], P('grp', 'kv'), parts along dimension 0, may hold values from -32 to 32
- in_gain: bfloat16 [4096], P('kv'), may hold values from 0.099609375 to 1.8984375
- query_weight: bfloat16 [4096, 4096], P('kv', 'tp'), may hold values from -0.09375 to 0.09375
- key_weight: bfloat16 [4096, 4096], P('kv', 'tp'), may hold values from -0.09375 to 0.09375
- value_weight: bfloat16 [4096, 8192], P('kv', 'tp'), may hold values from -0.09375 to 0.09375
- outgate_weight: bfloat16 [4096, 8192], P('kv', 'tp'), may hold values from -0.09375 to 0.09375
- input_gate_weight: bfloat16 [4096, 32], P('kv', 'tp'), may hold values from -0.09375 to 0.09375
- forget_gate_weight: bfloat16 [4096, 32], P('kv', 'tp'), may hold values from -0.09375 to 0.09375
- forget_bias: float32 [32], P('tp'), may hold values from -1 to 3
- state_matrix: float32 [256, 32, 128, 256], P(('grp', 'kv'), 'tp'), parts along dimension 0, may hold values from -3 to 3
- state_norm: float32 [256, 32, 128], P(('grp', 'kv'), 'tp'), parts along dimension 0, may hold values from -6 to 6
- state_max: float32 [256, 32], P(('grp', 'kv'), 'tp'), parts along dimension 0, may hold values from -1 to 1
- head_gain: bfloat16 [8192], P('tp'), may hold values from 0.099609375 to 1.8984375
- out_weight: bfloat16 [8192, 4096], P('tp', 'kv'), may hold values from -0.0625 to 0.0625
- mix_gain: bfloat16 [4096], P('kv'), may hold values from 0.099609375 to 1.8984375
- up_weight: bfloat16 [4096, 16384], P('kv', 'tp'), may hold values from -0.09375 to 0.09375
- down_weight: bfloat16 [16384, 4096], P('tp', 'kv'), may hold values from -0.046875 to 0.046875
Outputs:
- mixed_out: bfloat16 [256, 4096], P('grp', 'kv'), parts along dimension 0
- new_matrix: float32 [256, 32, 128, 256], P(('grp', 'kv'), 'tp'), parts along dimension 0
- new_norm: float32 [256, 32, 128], P(('grp', 'kv'), 'tp'), parts along dimension 0
- new_max: float32 [256, 32], P(('grp', 'kv'), 'tp'), parts along dimension 0
There are 2 independent parts, one for each index of `grp`. A program takes and returns all parts, laid end to end along the dimension named above; an argument that names none is the same for every part. Nothing has to cross between parts.
All inputs are finite; a program needn't handle non-finite values.
Results may differ from a plain program's by a relative error of at most 0.019.
Values may be sent and summed in bfloat16 or wider, within the bound.
A program may use at most 192 MiB of HBM per device.

v0:
```python
import jax
import jax.numpy as jnp
from jax import lax
from jax.sharding import PartitionSpec as P

D = 4096
DQK = 128
DV = 256
epsilon = 1e-06


def per_device(
    x_rows,
    in_gain,
    query_weight,
    key_weight,
    value_weight,
    outgate_weight,
    input_gate_weight,
    forget_gate_weight,
    forget_bias,
    state_matrix,
    state_norm,
    state_max,
    head_gain,
    out_weight,
    mix_gain,
    up_weight,
    down_weight,
):
    xfull = x_rows.astype(jnp.float32)
    partial_squares = jnp.sum(xfull * xfull, axis=1)
    scaled = (xfull * in_gain.astype(jnp.float32)).astype(jnp.bfloat16)
    gate_columns = jnp.concatenate([input_gate_weight, forget_gate_weight], axis=1)

    def product(weight):
        return jnp.dot(scaled, weight, preferred_element_type=jnp.float32)

    query_part, key_part, value_part, outgate_part, gate_part, squares = (
        lax.psum_scatter(product(query_weight), "kv", scatter_dimension=0, tiled=True),
        lax.psum_scatter(product(key_weight), "kv", scatter_dimension=0, tiled=True),
        lax.psum_scatter(product(value_weight), "kv", scatter_dimension=0, tiled=True),
        lax.psum_scatter(product(outgate_weight), "kv", scatter_dimension=0, tiled=True),
        lax.psum_scatter(product(gate_columns), "kv", scatter_dimension=0, tiled=True),
        lax.psum_scatter(partial_squares, "kv", scatter_dimension=0, tiled=True),
    )
    scale = lax.rsqrt(squares / D + epsilon)[:, None]
    row_count = state_max.shape[0]
    head_count = state_max.shape[1]

    def rounded(partial_value):
        return lax.optimization_barrier((partial_value * scale).astype(jnp.bfloat16)).astype(
            jnp.float32
        )

    query = rounded(query_part).reshape(row_count, head_count, DQK) * DQK ** (-0.5)
    keys = rounded(key_part).reshape(row_count, head_count, DQK)
    values = rounded(value_part).reshape(row_count, head_count, DV)
    outgate = rounded(outgate_part).reshape(row_count, head_count, DV)
    gates = gate_part * scale
    igate = gates[:, :head_count]
    fgate = gates[:, head_count:]
    log_forget = jax.nn.log_sigmoid(fgate + forget_bias[None, :])
    new_max = jnp.maximum(log_forget + state_max, igate)
    fdecay = jnp.exp(log_forget + state_max - new_max)
    idecay = jnp.exp(igate - new_max)
    new_matrix = fdecay[:, :, None, None] * state_matrix + idecay[:, :, None, None] * (
        keys[:, :, :, None] * values[:, :, None, :]
    )
    new_norm = fdecay[:, :, None] * state_norm + idecay[:, :, None] * keys
    numer = jnp.einsum("bhd,bhde->bhe", query, new_matrix, precision=lax.Precision.HIGHEST)
    denom = jnp.sum(query * new_norm, axis=-1)
    readout = numer / jnp.maximum(jnp.abs(denom), jnp.exp(-new_max))[:, :, None]
    normed = readout * lax.rsqrt(jnp.mean(readout * readout, axis=-1, keepdims=True) + epsilon)
    normed = normed * head_gain.astype(jnp.float32).reshape(head_count, DV)
    merged = (
        (jax.nn.sigmoid(outgate) * normed).reshape(row_count, head_count * DV).astype(jnp.bfloat16)
    )
    branch = jnp.dot(
        lax.all_gather(merged, "kv", axis=0, tiled=True),
        out_weight,
        preferred_element_type=jnp.float32,
    )
    branch = lax.psum(branch, "tp")
    resid = lax.optimization_barrier((xfull + branch).astype(jnp.bfloat16)).astype(jnp.float32)
    partial_two = jnp.sum(resid * resid, axis=1)
    scaled_two = (resid * mix_gain.astype(jnp.float32)).astype(jnp.bfloat16)
    up_part = jnp.dot(scaled_two, up_weight, preferred_element_type=jnp.float32)
    up_total, squares_two = (
        lax.psum_scatter(up_part, "kv", scatter_dimension=0, tiled=True),
        lax.psum_scatter(partial_two, "kv", scatter_dimension=0, tiled=True),
    )
    scale_two = lax.rsqrt(squares_two / D + epsilon)[:, None]
    hidden = jnp.square(jax.nn.relu(up_total * scale_two)).astype(jnp.bfloat16)
    down = jnp.dot(
        lax.all_gather(hidden, "kv", axis=0, tiled=True),
        down_weight,
        preferred_element_type=jnp.float32,
    )
    down = lax.psum(down.astype(jnp.bfloat16), "tp").astype(jnp.float32)
    mixed_out = (resid + down).astype(jnp.bfloat16)
    return (mixed_out, new_matrix, new_norm, new_max)


def solution(mesh):
    placed = (
        P("grp", "kv"),
        P("kv"),
        P("kv", "tp"),
        P("kv", "tp"),
        P("kv", "tp"),
        P("kv", "tp"),
        P("kv", "tp"),
        P("kv", "tp"),
        P("tp"),
        P(("grp", "kv"), "tp", None, None),
        P(("grp", "kv"), "tp", None),
        P(("grp", "kv"), "tp"),
        P("tp"),
        P("tp", "kv"),
        P("kv"),
        P("kv", "tp"),
        P("tp", "kv"),
    )
    return jax.shard_map(
        per_device,
        mesh=mesh,
        in_specs=placed,
        out_specs=(
            P("grp", "kv"),
            P(("grp", "kv"), "tp", None, None),
            P(("grp", "kv"), "tp", None),
            P(("grp", "kv"), "tp"),
        ),
        check_vma=False,
    )
```

profile of v0, /device:TPU:0, one launch (start us, length us, event | category | flops | bytes accessed | tf_op | source)
XLA Modules:
  0.0 355.6 jit_solution(17088462818694971066)
XLA Ops:
  7.2 0.8 convert_element_type.61
  8.1 1.8 fusion.14
  10.0 2.2 fusion.16
  12.3 3.0 fusion.12
  15.3 4.0 %fusion.10 = f32[128,2048]{1,0:T(8,128)} fusion(bf16[1024,2048]{1,0:T(8,128)(2,1)} %param.21, bf16[128,1024]{1,0:T(8,128)(2,1)} %param.17, f32[1024]{0:T(1024)S(1)} %convert_element_type.61), kind=kOutput, calls=%fused_computation.30 | convolution fusion | flops 537264128 | bytes 5509120 | tf_op jit(solution)/shard_map/dot_general | solution.py:37
  19.4 3.9 %fusion.18 = f32[128,2048]{1,0:T(8,128)} fusion(bf16[1024,2048]{1,0:T(8,128)(2,1)} %param.22, bf16[128,1024]{1,0:T(8,128)(2,1)S(1)} %copy-done.2, f32[1024]{0:T(1024)S(1)} %convert_element_type.61), kind=kOutput, calls=%fused_computation.34 | convolution fusion | flops 537264128 | bytes 5509120 | tf_op jit(solution)/shard_map/dot_general | solution.py:37
  23.5 0.6 dynamic-slice
  24.9 13.4 %all-reduce = f32[128]{0:T(128)S(1)} all-reduce(f32[128]{0:T(128)S(1)} %fusion.1), channel_id=3, replica_groups=mesh['grp'=2,'kv'=4,'tp'=4] {'kv'}, use_global_device_ids=true, to_apply=%region_2.0.clone | all-reduce | flops 128 | bytes 1024
  38.4 0.8 broadcast_multiply_fusion
  39.3 15.9 %reduce-scatter.11.cloned.1.call-done = f32[32,1024]{1,0:T(8,128)} async-done(((f32[128,1024]{1,0:T(8,128)}), f32[32,1024]{1,0:T(8,128)}) %reduce-scatter.11.cloned.1.call-update) | async-done | bytes 131088 | tf_op jit(solution)/shard_map/reduce_scatter | solution.py:40
  55.2 22.4 %reduce-scatter.13.cloned.1.call-done = f32[32,1024]{1,0:T(8,128)} async-done(((f32[128,1024]{1,0:T(8,128)}), f32[32,1024]{1,0:T(8,128)}) %reduce-scatter.13.cloned.1.call-update) | async-done | bytes 131088 | tf_op jit(solution)/shard_map/reduce_scatter | solution.py:41
  77.6 1.1 multiply_convert_fusion.3
  79.1 26.9 %reduce-scatter.15.cloned.1.call-done = f32[32,2048]{1,0:T(8,128)} async-done(((f32[128,2048]{1,0:T(8,128)}), f32[32,2048]{1,0:T(8,128)}) %reduce-scatter.15.cloned.1.call-update) | async-done | bytes 262160 | tf_op jit(solution)/shard_map/reduce_scatter | solution.py:42
  105.9 27.9 %reduce-scatter.9.cloned.1.call-done = f32[32,2048]{1,0:T(8,128)} async-done(((f32[128,2048]{1,0:T(8,128)}), f32[32,2048]{1,0:T(8,128)}) %reduce-scatter.9.cloned.1.call-update) | async-done | bytes 262160 | tf_op jit(solution)/shard_map/reduce_scatter | solution.py:43
  133.9 1.1 multiply_convert_fusion.1
  135.2 24.5 %multiply_add_fusion = f32[32,8,128,256]{3,2,1,0:T(8,128)} fusion(f32[32,8,128,256]{3,2,1,0:T(8,128)} %param.26, f32[32,8,256]{2,1,0:T(8,128)S(1)} %bitcast.45, f32[32,8,128]{2,1,0:T(8,128)S(1)} %bitcast.44, f32[32,8]{1,0:T(8,128)S(1)} %subtract_exponential_fusion, f32[32,8]{1,0:T(8,128)S(1)} %get-tuple-element.8), kind=kLoop, calls=%fused_computation | loop fusion | flops 33554432 | bytes 67504128 | tf_op jit(solution)/shard_map/add | solution.py:67
  159.8 19.8 %fusion.31 = f32[32,8,1,256]{3,2,1,0:T(1,128)S(1)} fusion(f32[32,8,128,1]{2,3,1,0:T(1,128)S(1)} %bitcast.43, f32[32,8,128,256]{3,2,1,0:T(8,128)} %multiply_add_fusion), kind=kOutput, calls=%fused_computation.56 | convolution fusion | flops 100663296 | bytes 33947648 | tf_op jit(solution)/shard_map/bhd,bhde->bhe/dot_general | solution.py:71
  179.6 0.2 multiply_reduce_fusion
  179.8 0.1 fusion.8
  179.9 16.0 %all_gather.6 = bf16[128,2048]{1,0:T(8,128)(2,1)S(1)} all-gather(bf16[32,2048]{1,0:T(8,128)(2,1)S(1)} %bitcast.47), channel_id=1, replica_groups=mesh['grp'=2,'kv'=4,'tp'=4] {'kv'}, dimensions={0}, use_global_device_ids=true | all-gather | bytes 655360 | tf_op jit(solution)/shard_map/all_gather | solution.py:80
  195.9 1.6 fusion.32
  197.5 31.9 %all-reduce.5.cloned.1.call-done = f32[128,1024]{1,0:T(8,128)} async-done(((f32[128,1024]{1,0:T(8,128)}), f32[128,1024]{1,0:T(8,128)}) %all-reduce.5.cloned.1.call-update) | async-done | bytes 524304 | tf_op jit(solution)/shard_map/psum | solution.py:84
  229.4 1.1 fusion.2
  230.5 6.0 %fusion.6 = f32[128,4096]{1,0:T(8,128)} fusion(bf16[1024,4096]{1,0:T(8,128)(2,1)} %param.32, bf16[128,1024]{1,0:T(8,128)(2,1)S(1)} %fusion.2, f32[1024]{0:T(1024)S(1)} %convert_element_type.73), kind=kOutput, calls=%fused_computation.15 | convolution fusion | flops 1074135040 | bytes 10752000 | tf_op jit(solution)/shard_map/dot_general | solution.py:88
  236.7 11.8 %all-reduce.1 = f32[128]{0:T(128)S(1)} all-reduce(f32[128]{0:T(128)S(1)} %fusion.4), channel_id=9, replica_groups=mesh['grp'=2,'kv'=4,'tp'=4] {'kv'}, use_global_device_ids=true, to_apply=%region_12.13.clone | all-reduce | flops 128 | bytes 1024
  248.6 31.8 %reduce-scatter.17.cloned.1.call-done = f32[32,4096]{1,0:T(8,128)} async-done(((f32[128,4096]{1,0:T(8,128)}), f32[32,4096]{1,0:T(8,128)}) %reduce-scatter.17.cloned.1.call-update) | async-done | bytes 524304 | tf_op jit(solution)/shard_map/reduce_scatter | solution.py:90
  280.5 1.9 multiply_convert_fusion
  282.4 27.4 %all-gather.2.cloned.1.call-done = bf16[128,4096]{1,0:T(8,128)(2,1)} async-done(((bf16[32,4096]{1,0:T(8,128)(2,1)}), bf16[128,4096]{1,0:T(8,128)(2,1)}) %all-gather.2.cloned.1.call-update) | async-done | bytes 1048592 | tf_op jit(solution)/shard_map/all_gather | solution.py:96
  309.8 5.7 %convolution_convert_fusion = bf16[128,1024]{1,0:T(8,128)(2,1)} fusion(bf16[128,4096]{1,0:T(8,128)(2,1)} %all-gather.2.cloned.1.call-done, bf16[4096,1024]{1,0:T(8,128)(2,1)} %param.33), kind=kOutput, calls=%fused_computation.1 | convolution fusion | flops 1073872896 | bytes 9699328 | tf_op jit(solution)/shard_map/dot_general | solution.py:95
  315.5 0.7 copy.28
  316.2 31.2 %all-reduce.7.cloned.1.call-done = bf16[128,1024]{1,0:T(8,128)(2,1)} async-done(((bf16[128,1024]{1,0:T(8,128)(2,1)}), bf16[128,1024]{1,0:T(8,128)(2,1)}) %all-reduce.7.cloned.1.call-update) | async-done | bytes 262160 | tf_op jit(solution)/shard_map/psum | solution.py:100
  347.3 1.7 fusion.5
  (62 shorter events, 1.8 us)
Async XLA Ops:
  7.2 2.8 copy-start
  7.2 12.2 %copy-start.2 = (bf16[128,1024]{1,0:T(8,128)(2,1)S(1)}, bf16[128,1024]{1,0:T(8,128)(2,1)}, u32[]{:S(2)}) copy-start(bf16[128,1024]{1,0:T(8,128)(2,1)} %param.17) | copy-start | bytes 786436
  7.2 31.2 %reduce-scatter.19.cloned.1.call-start = ((), (), s32[]{:S(2)}) async-start(), calls=%async_computation.14 | async-start | bytes 81920 | tf_op jit(solution)/shard_map/reduce_scatter | solution.py:44
  9.9 45.3 %reduce-scatter.11.cloned.1.call-start = ((), (), s32[]{:S(2)}) async-start(), calls=%async_computation.7 | async-start | bytes 655360 | tf_op jit(solution)/shard_map/reduce_scatter | solution.py:40
  12.2 11.3 %copy-start.10 = (u32[32]{0:T(128)S(1)}, u32[32]{0:T(128)}, u32[]{:S(2)}) copy-start(u32[32]{0:T(128)} %constant.23) | copy-start | bytes 388
  12.2 12.5 %copy-start.6 = (bf16[2048]{0:T(1024)(128)(2,1)S(1)}, bf16[2048]{0:T(1024)(128)(2,1)}, u32[]{:S(2)}) copy-start(bf16[2048]{0:T(1024)(128)(2,1)} %param.29) | copy-start | bytes 12292
  12.2 12.6 %copy-start.7 = (f32[32,8]{0,1:T(8,128)S(1)}, f32[32,8]{0,1:T(8,128)}, u32[]{:S(2)}) copy-start(f32[32,8]{0,1:T(8,128)} %param.28) | copy-start | bytes 3076
  12.2 26.9 %copy-start.9 = (f32[8]{0:T(128)S(1)}, f32[8]{0:T(128)}, u32[]{:S(2)}) copy-start(f32[8]{0:T(128)} %param.25) | copy-start | bytes 100
  12.3 65.4 %reduce-scatter.13.cloned.1.call-start = ((), (), s32[]{:S(2)}) async-start(), calls=%async_computation.8 | async-start | bytes 655360 | tf_op jit(solution)/shard_map/reduce_scatter | solution.py:41
  15.3 63.5 %copy-start.5 = (f32[32,8,128]{2,1,0:T(8,128)S(1)}, f32[32,8,128]{2,1,0:T(8,128)}, u32[]{:S(2)}) copy-start(f32[32,8,128]{2,1,0:T(8,128)} %param.27) | copy-start | bytes 393220
  15.3 90.7 %reduce-scatter.15.cloned.1.call-start = ((), (), s32[]{:S(2)}) async-start(), calls=%async_computation.9 | async-start | bytes 1310720 | tf_op jit(solution)/shard_map/reduce_scatter | solution.py:42
  19.3 114.6 %reduce-scatter.9.cloned.1.call-start = ((), (), s32[]{:S(2)}) async-start(), calls=%async_computation.6 | async-start | bytes 1310720 | tf_op jit(solution)/shard_map/reduce_scatter | solution.py:43
  23.3 206.1 %all-reduce.5.cloned.1.call-start = ((), (), s32[]{:S(2)}) async-start(), calls=%async_computation.10 | async-start | bytes 1048576 | tf_op jit(solution)/shard_map/psum | solution.py:84
  78.9 80.8 %copy-start.4 = (f32[32,8,128]{2,1,0:T(8,128)}, f32[32,8,128]{2,1,0:T(8,128)S(1)}, u32[]{:S(2)}) copy-start(f32[32,8,128]{2,1,0:T(8,128)S(1)} %multiply_add_fusion.1) | copy-start | bytes 393220
  159.7 36.1 %copy-start.3 = (bf16[2048,1024]{1,0:T(8,128)(2,1)S(1)}, bf16[2048,1024]{1,0:T(8,128)(2,1)}, u32[]{:S(2)}) copy-start(bf16[2048,1024]{1,0:T(8,128)(2,1)} %param.30) | copy-start | bytes 12582916
  159.7 37.8 %copy-start.8 = (bf16[1024]{0:T(1024)(128)(2,1)S(1)}, bf16[1024]{0:T(1024)(128)(2,1)}, u32[]{:S(2)}) copy-start(bf16[1024]{0:T(1024)(128)(2,1)} %param.31) | copy-start | bytes 6148
  197.5 83.0 %reduce-scatter.17.cloned.1.call-start = ((), (), s32[]{:S(2)}) async-start(), calls=%async_computation.11 | async-start | bytes 2621440 | tf_op jit(solution)/shard_map/reduce_scatter | solution.py:90
  236.5 73.3 %all-gather.2.cloned.1.call-start = ((), (), s32[]{:S(2)}) async-start(), calls=%async_computation.12 | async-start | bytes 1310720 | tf_op jit(solution)/shard_map/all_gather | solution.py:96
  282.4 66.7 %copy-start.1 = (bf16[1024,1024]{1,0:T(8,128)(2,1)S(1)}, bf16[1024,1024]{1,0:T(8,128)(2,1)}, u32[]{:S(2)}) copy-start(bf16[1024,1024]{1,0:T(8,128)(2,1)} %param.19) | copy-start | bytes 6291460
  282.4 65.0 %all-reduce.7.cloned.1.call-start = ((), (), s32[]{:S(2)}) async-start(), calls=%async_computation.13 | async-start | bytes 524288 | tf_op jit(solution)/shard_map/psum | solution.py:100
Sparse Core Ops, SparseCore 0:
  10.8 22.0 reduce-scatter.18
  35.2 19.9 reduce-scatter.10
  57.5 20.1 reduce-scatter.12
  80.3 25.5 reduce-scatter.14
  108.1 25.7 reduce-scatter.8
  197.6 31.7 all-reduce.4
  236.6 43.7 reduce-scatter.16
  282.6 27.1 all-gather.1
  315.6 31.6 all-reduce.6
where the time goes:
time: 356 us
  waiting for transfers between devices  216 us (61%)
  matrix products  47.9 us (13%)
  blocking collectives  41.2 us (12%)
  other arithmetic  34.2 us (10%)
  between operations  14.8 us (4%)
    psum x1, waiting for transfers between devices, per_device(): branch = lax.psum(branch, 'tp')  31.9 us
    reduce_scatter x1, waiting for transfers between devices, per_device(): lax.psum_scatter(up_part, 'kv', scatter_dimension=0, tiled=True)  31.8 us
    psum x1, waiting for transfers between devices, per_device(): down = lax.psum(down.astype(jnp.bfloat16), 'tp').astype(jnp.float32)  31.2 us
    reduce_scatter x1, waiting for transfers between devices, per_device(): lax.psum_scatter(product(outgate_weight), 'kv', scatter_dimension=0, tile...  27.9 us
    all_gather x1, waiting for transfers between devices, per_device(): lax.all_gather(hidden, 'kv', axis=0, tiled=True)  27.4 us
    reduce_scatter x1, waiting for transfers between devices, per_device(): lax.psum_scatter(product(value_weight), 'kv', scatter_dimension=0, tiled=...  26.9 us
    unnamed x2, blocking collectives  25.3 us
    add x1, other arithmetic, per_device(): fdecay[:, :, None, None] * state_matrix  24.5 us
  transfers between devices with their start and end apart: 9, of which 8 were waited for; matrix products, arithmetic and copies ran while one was open for 5% of the time, Pallas kernels for 0%

commit v1 on v0

--- a/solution.py
+++ b/solution.py
@@ -97,7 +97,7 @@
         down_weight,
         preferred_element_type=jnp.float32,
     )
-    down = lax.psum(down.astype(jnp.bfloat16), "tp").astype(jnp.float32)
+    down = jnp.sum(lax.all_gather(down.astype(jnp.bfloat16), "tp"), axis=0).astype(jnp.float32)
     mixed_out = (resid + down).astype(jnp.bfloat16)
     return (mixed_out, new_matrix, new_norm, new_max)
 

time: 356 us -> 341 us (0.958)
  waiting for transfers between devices: 216 us -> 200 us
    psum x1 -> x0, waiting for transfers between devices: 31.2 us -> none  [per_device(): down = lax.psum(down.astype(jnp.bfloat16), 'tp').astype(jnp.float32)]
    all_gather x0 -> x1, waiting for transfers between devices: none -> 15.6 us  [per_device(): lax.all_gather(down.astype(jnp.bfloat16), 'tp')]
where the time goes in v1:
time: 341 us; the launch traced here: 340 us
  waiting for transfers between devices  200 us (59%)
  matrix products  47.9 us (14%)
  blocking collectives  41.2 us (12%)
  other arithmetic  34.7 us (10%)
  between operations  14.8 us (4%)
    psum x1, waiting for transfers between devices, per_device(): branch = lax.psum(branch, 'tp')  31.9 us
    reduce_scatter x1, waiting for transfers between devices, per_device(): lax.psum_scatter(up_part, 'kv', scatter_dimension=0, tiled=True)  31.8 us
    reduce_scatter x1, waiting for transfers between devices, per_device(): lax.psum_scatter(product(outgate_weight), 'kv', scatter_dimension=0, tile...  27.9 us
    all_gather x1, waiting for transfers between devices, per_device(): lax.all_gather(hidden, 'kv', axis=0, tiled=True)  27.4 us
    reduce_scatter x1, waiting for transfers between devices, per_device(): lax.psum_scatter(product(value_weight), 'kv', scatter_dimension=0, tiled=...  26.9 us
    unnamed x2, blocking collectives  25.3 us
    add x1, other arithmetic, per_device(): fdecay[:, :, None, None] * state_matrix  24.5 us
    reduce_scatter x1, waiting for transfers between devices, per_device(): lax.psum_scatter(product(key_weight), 'kv', scatter_dimension=0, tiled=True)  22.4 us
  transfers between devices with their start and end apart: 9, of which 8 were waited for; matrix products, arithmetic and copies ran while one was open for 5% of the time, Pallas kernels for 0%

profile of v1, /device:TPU:0, one launch (start us, length us, event | category | flops | bytes accessed | tf_op | source)
XLA Modules:
  0.0 340.5 jit_solution(3619572743938683975)
XLA Ops:
  7.2 0.8 convert_element_type.63
  8.1 1.8 fusion.14
  10.0 2.2 fusion.16
  12.3 3.0 fusion.12
  15.3 4.0 %fusion.10 = f32[128,2048]{1,0:T(8,128)} fusion(bf16[1024,2048]{1,0:T(8,128)(2,1)} %param.21, bf16[128,1024]{1,0:T(8,128)(2,1)} %param.17, f32[1024]{0:T(1024)S(1)} %convert_element_type.63), kind=kOutput, calls=%fused_computation.30 | convolution fusion | flops 537264128 | bytes 5509120 | tf_op jit(solution)/shard_map/dot_general | solution.py:37
  19.4 3.9 %fusion.18 = f32[128,2048]{1,0:T(8,128)} fusion(bf16[1024,2048]{1,0:T(8,128)(2,1)} %param.22, bf16[128,1024]{1,0:T(8,128)(2,1)S(1)} %copy-done.2, f32[1024]{0:T(1024)S(1)} %convert_element_type.63), kind=kOutput, calls=%fused_computation.34 | convolution fusion | flops 537264128 | bytes 5509120 | tf_op jit(solution)/shard_map/dot_general | solution.py:37
  23.5 0.6 dynamic-slice
  24.9 13.4 %all-reduce = f32[128]{0:T(128)S(1)} all-reduce(f32[128]{0:T(128)S(1)} %fusion.1), channel_id=4, replica_groups=mesh['grp'=2,'kv'=4,'tp'=4] {'kv'}, use_global_device_ids=true, to_apply=%region_2.0.clone | all-reduce | flops 128 | bytes 1024
  38.4 0.8 broadcast_multiply_fusion
  39.3 15.9 %reduce-scatter.11.cloned.1.call-done = f32[32,1024]{1,0:T(8,128)} async-done(((f32[128,1024]{1,0:T(8,128)}), f32[32,1024]{1,0:T(8,128)}) %reduce-scatter.11.cloned.1.call-update) | async-done | bytes 131088 | tf_op jit(solution)/shard_map/reduce_scatter | solution.py:40
  55.2 22.4 %reduce-scatter.13.cloned.1.call-done = f32[32,1024]{1,0:T(8,128)} async-done(((f32[128,1024]{1,0:T(8,128)}), f32[32,1024]{1,0:T(8,128)}) %reduce-scatter.13.cloned.1.call-update) | async-done | bytes 131088 | tf_op jit(solution)/shard_map/reduce_scatter | solution.py:41
  77.6 1.1 multiply_convert_fusion.3
  79.1 26.9 %reduce-scatter.15.cloned.1.call-done = f32[32,2048]{1,0:T(8,128)} async-done(((f32[128,2048]{1,0:T(8,128)}), f32[32,2048]{1,0:T(8,128)}) %reduce-scatter.15.cloned.1.call-update) | async-done | bytes 262160 | tf_op jit(solution)/shard_map/reduce_scatter | solution.py:42
  105.9 27.9 %reduce-scatter.9.cloned.1.call-done = f32[32,2048]{1,0:T(8,128)} async-done(((f32[128,2048]{1,0:T(8,128)}), f32[32,2048]{1,0:T(8,128)}) %reduce-scatter.9.cloned.1.call-update) | async-done | bytes 262160 | tf_op jit(solution)/shard_map/reduce_scatter | solution.py:43
  133.9 1.1 multiply_convert_fusion.1
  135.2 24.5 %multiply_add_fusion = f32[32,8,128,256]{3,2,1,0:T(8,128)} fusion(f32[32,8,128,256]{3,2,1,0:T(8,128)} %param.26, f32[32,8,256]{2,1,0:T(8,128)S(1)} %bitcast.46, f32[32,8,128]{2,1,0:T(8,128)S(1)} %bitcast.45, f32[32,8]{1,0:T(8,128)S(1)} %subtract_exponential_fusion, f32[32,8]{1,0:T(8,128)S(1)} %get-tuple-element.8), kind=kLoop, calls=%fused_computation | loop fusion | flops 33554432 | bytes 67504128 | tf_op jit(solution)/shard_map/add | solution.py:67
  159.8 19.8 %fusion.31 = f32[32,8,1,256]{3,2,1,0:T(1,128)S(1)} fusion(f32[32,8,128,1]{2,3,1,0:T(1,128)S(1)} %bitcast.44, f32[32,8,128,256]{3,2,1,0:T(8,128)} %multiply_add_fusion), kind=kOutput, calls=%fused_computation.56 | convolution fusion | flops 100663296 | bytes 33947648 | tf_op jit(solution)/shard_map/bhd,bhde->bhe/dot_general | solution.py:71
  179.6 0.2 multiply_reduce_fusion
  179.9 16.0 %all_gather.12 = bf16[128,2048]{1,0:T(8,128)(2,1)S(1)} all-gather(bf16[32,2048]{1,0:T(8,128)(2,1)S(1)} %bitcast.49), channel_id=1, replica_groups=mesh['grp'=2,'kv'=4,'tp'=4] {'kv'}, dimensions={0}, use_global_device_ids=true | all-gather | bytes 655360 | tf_op jit(solution)/shard_map/all_gather | solution.py:80
  195.9 1.6 fusion.32
  197.5 31.9 %all-reduce.4.cloned.1.call-done = f32[128,1024]{1,0:T(8,128)} async-done(((f32[128,1024]{1,0:T(8,128)}), f32[128,1024]{1,0:T(8,128)}) %all-reduce.4.cloned.1.call-update) | async-done | bytes 524304 | tf_op jit(solution)/shard_map/psum | solution.py:84
  229.4 1.1 fusion.2
  230.5 6.0 %fusion.6 = f32[128,4096]{1,0:T(8,128)} fusion(bf16[1024,4096]{1,0:T(8,128)(2,1)} %param.32, bf16[128,1024]{1,0:T(8,128)(2,1)S(1)} %fusion.2, f32[1024]{0:T(1024)S(1)} %convert_element_type.75), kind=kOutput, calls=%fused_computation.15 | convolution fusion | flops 1074135040 | bytes 10752000 | tf_op jit(solution)/shard_map/dot_general | solution.py:88
  236.7 11.8 %all-reduce.1 = f32[128]{0:T(128)S(1)} all-reduce(f32[128]{0:T(128)S(1)} %fusion.4), channel_id=10, replica_groups=mesh['grp'=2,'kv'=4,'tp'=4] {'kv'}, use_global_device_ids=true, to_apply=%region_12.13.clone | all-reduce | flops 128 | bytes 1024
  248.6 31.8 %reduce-scatter.17.cloned.1.call-done = f32[32,4096]{1,0:T(8,128)} async-done(((f32[128,4096]{1,0:T(8,128)}), f32[32,4096]{1,0:T(8,128)}) %reduce-scatter.17.cloned.1.call-update) | async-done | bytes 524304 | tf_op jit(solution)/shard_map/reduce_scatter | solution.py:90
  280.5 1.9 multiply_convert_fusion
  282.4 27.4 %all-gather.4.cloned.1.call-done = bf16[128,4096]{1,0:T(8,128)(2,1)} async-done(((bf16[32,4096]{1,0:T(8,128)(2,1)}), bf16[128,4096]{1,0:T(8,128)(2,1)}) %all-gather.4.cloned.1.call-update) | async-done | bytes 1048592 | tf_op jit(solution)/shard_map/all_gather | solution.py:96
  309.8 5.7 %convolution_convert_fusion = bf16[128,1024]{1,0:T(8,128)(2,1)} fusion(bf16[128,4096]{1,0:T(8,128)(2,1)} %all-gather.4.cloned.1.call-done, bf16[4096,1024]{1,0:T(8,128)(2,1)} %param.33), kind=kOutput, calls=%fused_computation.1 | convolution fusion | flops 1073872896 | bytes 9699328 | tf_op jit(solution)/shard_map/dot_general | solution.py:95
  315.5 0.7 copy.28
  316.2 15.6 %all-gather.6.cloned.1.call-done = bf16[512,1024]{1,0:T(8,128)(2,1)} async-done(((bf16[128,1024]{1,0:T(8,128)(2,1)}), bf16[512,1024]{1,0:T(8,128)(2,1)}) %all-gather.6.cloned.1.call-update) | async-done | bytes 1048592 | tf_op jit(solution)/shard_map/all_gather | solution.py:100
  331.8 1.4 reduce_sum.52
  333.2 0.8 fusion.5
  (63 shorter events, 1.9 us)
Async XLA Ops:
  7.2 2.8 copy-start
  7.2 12.2 %copy-start.2 = (bf16[128,1024]{1,0:T(8,128)(2,1)S(1)}, bf16[128,1024]{1,0:T(8,128)(2,1)}, u32[]{:S(2)}) copy-start(bf16[128,1024]{1,0:T(8,128)(2,1)} %param.17) | copy-start | bytes 786436
  7.2 31.2 %reduce-scatter.19.cloned.1.call-start = ((), (), s32[]{:S(2)}) async-start(), calls=%async_computation.14 | async-start | bytes 81920 | tf_op jit(solution)/shard_map/reduce_scatter | solution.py:44
  9.9 45.3 %reduce-scatter.11.cloned.1.call-start = ((), (), s32[]{:S(2)}) async-start(), calls=%async_computation.7 | async-start | bytes 655360 | tf_op jit(solution)/shard_map/reduce_scatter | solution.py:40
  12.2 11.3 %copy-start.10 = (u32[32]{0:T(128)S(1)}, u32[32]{0:T(128)}, u32[]{:S(2)}) copy-start(u32[32]{0:T(128)} %constant.25) | copy-start | bytes 388
  12.2 12.5 %copy-start.6 = (bf16[2048]{0:T(1024)(128)(2,1)S(1)}, bf16[2048]{0:T(1024)(128)(2,1)}, u32[]{:S(2)}) copy-start(bf16[2048]{0:T(1024)(128)(2,1)} %param.29) | copy-start | bytes 12292
  12.2 12.6 %copy-start.7 = (f32[32,8]{0,1:T(8,128)S(1)}, f32[32,8]{0,1:T(8,128)}, u32[]{:S(2)}) copy-start(f32[32,8]{0,1:T(8,128)} %param.28) | copy-start | bytes 3076
  12.2 26.9 %copy-start.9 = (f32[8]{0:T(128)S(1)}, f32[8]{0:T(128)}, u32[]{:S(2)}) copy-start(f32[8]{0:T(128)} %param.25) | copy-start | bytes 100
  12.3 65.4 %reduce-scatter.13.cloned.1.call-start = ((), (), s32[]{:S(2)}) async-start(), calls=%async_computation.8 | async-start | bytes 655360 | tf_op jit(solution)/shard_map/reduce_scatter | solution.py:41
  15.3 63.5 %copy-start.5 = (f32[32,8,128]{2,1,0:T(8,128)S(1)}, f32[32,8,128]{2,1,0:T(8,128)}, u32[]{:S(2)}) copy-start(f32[32,8,128]{2,1,0:T(8,128)} %param.27) | copy-start | bytes 393220
  15.3 90.7 %reduce-scatter.15.cloned.1.call-start = ((), (), s32[]{:S(2)}) async-start(), calls=%async_computation.9 | async-start | bytes 1310720 | tf_op jit(solution)/shard_map/reduce_scatter | solution.py:42
  19.3 114.6 %reduce-scatter.9.cloned.1.call-start = ((), (), s32[]{:S(2)}) async-start(), calls=%async_computation.6 | async-start | bytes 1310720 | tf_op jit(solution)/shard_map/reduce_scatter | solution.py:43
  23.3 206.1 %all-reduce.4.cloned.1.call-start = ((), (), s32[]{:S(2)}) async-start(), calls=%async_computation.10 | async-start | bytes 1048576 | tf_op jit(solution)/shard_map/psum | solution.py:84
  78.9 80.8 %copy-start.4 = (f32[32,8,128]{2,1,0:T(8,128)}, f32[32,8,128]{2,1,0:T(8,128)S(1)}, u32[]{:S(2)}) copy-start(f32[32,8,128]{2,1,0:T(8,128)S(1)} %multiply_add_fusion.1) | copy-start | bytes 393220
  159.7 36.1 %copy-start.3 = (bf16[2048,1024]{1,0:T(8,128)(2,1)S(1)}, bf16[2048,1024]{1,0:T(8,128)(2,1)}, u32[]{:S(2)}) copy-start(bf16[2048,1024]{1,0:T(8,128)(2,1)} %param.30) | copy-start | bytes 12582916
  159.7 37.8 %copy-start.8 = (bf16[1024]{0:T(1024)(128)(2,1)S(1)}, bf16[1024]{0:T(1024)(128)(2,1)}, u32[]{:S(2)}) copy-start(bf16[1024]{0:T(1024)(128)(2,1)} %param.31) | copy-start | bytes 6148
  197.5 83.0 %reduce-scatter.17.cloned.1.call-start = ((), (), s32[]{:S(2)}) async-start(), calls=%async_computation.11 | async-start | bytes 2621440 | tf_op jit(solution)/shard_map/reduce_scatter | solution.py:90
  236.5 73.3 %all-gather.4.cloned.1.call-start = ((), (), s32[]{:S(2)}) async-start(), calls=%async_computation.12 | async-start | bytes 1310720 | tf_op jit(solution)/shard_map/all_gather | solution.py:96
  282.4 51.6 %copy-start.1 = (bf16[1024,1024]{1,0:T(8,128)(2,1)S(1)}, bf16[1024,1024]{1,0:T(8,128)(2,1)}, u32[]{:S(2)}) copy-start(bf16[1024,1024]{1,0:T(8,128)(2,1)} %param.19) | copy-start | bytes 6291460
  282.4 49.4 %all-gather.6.cloned.1.call-start = ((), (), s32[]{:S(2)}) async-start(), calls=%async_computation.13 | async-start | bytes 1310720 | tf_op jit(solution)/shard_map/all_gather | solution.py:100
Sparse Core Ops, SparseCore 0:
  10.8 22.0 reduce-scatter.18
  35.2 19.9 reduce-scatter.10
  57.5 20.1 reduce-scatter.12
  80.3 25.5 reduce-scatter.14
  108.1 25.7 reduce-scatter.8
  197.6 31.7 all-reduce.3
  236.6 43.7 reduce-scatter.16
  282.6 27.1 all-gather.3
  315.6 16.0 all-gather.5
